TPU v7x, 128 devices: a whole 4x4x4 slice. The times are simulated.
128 devices in a mesh: ep: 64 (over z, y, x), tp: 2 (over core).
Axes of the slice: x: 4, y: 4, z: 4, core: 2. Of those that a mesh axis runs over, the one named last changes fastest.
Arguments:
- inputs: bfloat16 [32768, 2048], P(('ep', 'tp')), may hold values from -6 to 6
- pre_gain: float32 [2048], replicated, may hold values from 0.5 to 8
- expert_ids: int32 [32768, 2], P(('ep', 'tp')), may hold values from 0 to 63, all different within a row; in each aligned block of 256 rows (0 to 255, 256 to 511, ...) at most 12 rows name the same one
- route_weights: float32 [32768, 2], P(('ep', 'tp')), may hold values from 0.05 to 1
- gate_proj: bfloat16 [64, 2048, 2048], P('ep', None, 'tp'), may hold values from -0.125 to 0.125
- up_proj: bfloat16 [64, 2048, 2048], P('ep', None, 'tp'), may hold values from -0.125 to 0.125
- down_proj: bfloat16 [64, 2048, 2048], P('ep', 'tp'), may hold values from -0.125 to 0.125
- post_gain: float32 [2048], replicated, may hold values from 0.1 to 1.9
Outputs:
- layer_out: bfloat16 [32768, 2048], P(('ep', 'tp'))
Inputs may be any that keep to these rules, and one draw needn't show every extreme that they name: `expert_ids`: each token names 2 different experts. Among the 256 tokens of one device (aligned blocks of rows) no expert is named by more than 12 tokens, and in every draw some expert is named by exactly 12 tokens of some device.
All inputs are finite; a program needn't handle non-finite values.
Results may differ from a plain program's by a relative error of at most 0.0095.
Values may be sent and summed in bfloat16 or wider, within the bound.
A program may use at most 128 MiB of HBM per device.

v0:
```python
import functools

import jax
import jax.numpy as jnp
from jax import lax
from jax.experimental import pallas as pl
from jax.experimental.pallas import tpu as pltpu
from jax.sharding import PartitionSpec as P

EPSILON = 1e-06
LIMIT = 7.0
ALPHA = 1.702
MESH = pl.DeviceIdType.MESH

N_EP = 64
CAP = 12
SLAB = 4
SLABS = CAP // SLAB
TILE = 256


def norm_rows(floats, gain):
    return floats * lax.rsqrt(jnp.mean(floats * floats, axis=-1, keepdims=True) + EPSILON) * gain


def offset_device(ep, o, sign):
    a, b, c = o % 4, (o // 4) % 4, o // 16
    ox, oy, oz = a, (b + a) % 4, (c + b) % 4
    x, y, z = ep % 4, (ep // 4) % 4, ep // 16
    return (
        ((z + sign * oz + 4) % 4) * 16 + ((y + sign * oy + 4) % 4) * 4 + (x + sign * ox + 4) % 4
    )


def kernel(
    chunks,
    x_ref,
    pre_ref,
    ids_ref,
    route_ref,
    gate_ref,
    up_ref,
    down_ref,
    post_ref,
    out_ref,
    x_buf,
    normed,
    place,
    pick0,
    pick1,
    send,
    recv,
    wg,
    wu,
    wd,
    rows,
    hidden,
    back,
    ret,
    total,
    load_sem,
    w_load,
    w_send,
    w_recv,
    s_send,
    s_recv,
    r_send,
    r_recv,
):
    ep = lax.axis_index("ep")
    tp = lax.axis_index("tp")
    tokens, width = x_buf.shape
    half = wg.shape[2]
    per = N_EP // chunks
    chunk_rows = per * CAP
    chunk_slabs = per * SLABS

    x_copy = pltpu.make_async_copy(x_ref, x_buf, load_sem)
    x_copy.start()
    weights = ((gate_ref, wg), (up_ref, wu), (down_ref, wd))
    for n, (source, target) in enumerate(weights):
        pltpu.make_async_copy(source, target.at[tp], w_load.at[n]).start()

    barrier = pltpu.get_barrier_semaphore()

    def greet(o, carry):
        pl.semaphore_signal(
            barrier, inc=1, device_id=((ep + o) % N_EP, tp), device_id_type=MESH
        )
        return carry

    lax.fori_loop(1, N_EP, greet, 0)
    pl.semaphore_signal(barrier, inc=1, device_id=(ep, 1 - tp), device_id_type=MESH)

    ids = ids_ref[...]
    route = route_ref[...]
    expert = lax.broadcasted_iota(jnp.int32, (N_EP, tokens), 0)
    hot0 = (expert == ids[0:1, :]).astype(jnp.bfloat16)
    hot1 = (expert == ids[1:2, :]).astype(jnp.bfloat16)
    row = lax.broadcasted_iota(jnp.int32, (tokens, tokens), 0)
    column = lax.broadcasted_iota(jnp.int32, (tokens, tokens), 1)
    before = (row < column).astype(jnp.bfloat16)
    count0 = jnp.dot(hot0, before, preferred_element_type=jnp.float32)
    count1 = jnp.dot(hot1, before, preferred_element_type=jnp.float32)
    hot0 = hot0.astype(jnp.float32)
    hot1 = hot1.astype(jnp.float32)
    count1 = count1 + jnp.sum(hot0, axis=1, keepdims=True)
    slot0 = jnp.sum(hot0 * count0, axis=0, keepdims=True)
    slot1 = jnp.sum(hot1 * count1, axis=0, keepdims=True)
    x_me, y_me, z_me = ep % 4, (ep // 4) % 4, ep // 16
    a = (ids % 4 - x_me + 4) % 4
    b = ((ids // 4) % 4 - y_me - a + 8) % 4
    c = (ids // 16 - z_me - b + 8) % 4
    order = (a + 4 * b + 16 * c).astype(jnp.float32) * float(CAP)
    target0 = order[0:1, :] + slot0
    target1 = order[1:2, :] + slot1
    slots = N_EP * CAP
    slot_rows = lax.broadcasted_iota(jnp.int32, (slots, tokens), 0).astype(jnp.float32)
    place[...] = jnp.where(
        (slot_rows == target0) | (slot_rows == target1), 1.0, 0.0
    ).astype(jnp.bfloat16)
    diagonal = row == column

    def upright(line):
        return jnp.sum(jnp.where(diagonal, line, 0.0), axis=1, keepdims=True)

    x_copy.wait()
    pre_gain = pre_ref[...]
    step_rows = 32

    def norm_step(i, carry):
        here = pl.ds(pl.multiple_of(i * step_rows, step_rows), step_rows)
        normed[here, :] = norm_rows(x_buf[here, :].astype(jnp.float32), pre_gain).astype(
            jnp.bfloat16
        )
        return carry

    lax.fori_loop(0, tokens // step_rows, norm_step, 0)

    pl.semaphore_wait(barrier, N_EP)

    def message(buffer, o):
        return buffer.at[pl.ds(o * SLABS, SLABS)]

    def outgoing(o):
        return pltpu.make_async_remote_copy(
            src_ref=message(send, o),
            dst_ref=message(recv, o),
            send_sem=s_send.at[o],
            recv_sem=s_recv.at[o],
            device_id=(offset_device(ep, o, 1), tp),
            device_id_type=MESH,
        )

    def returning(o):
        return pltpu.make_async_remote_copy(
            src_ref=message(back, o),
            dst_ref=message(ret, o),
            send_sem=r_send.at[o],
            recv_sem=r_recv.at[o],
            device_id=(offset_device(ep, o, -1), tp),
            device_id_type=MESH,
        )

    own_out = pltpu.make_async_copy(message(send, 0), message(recv, 0), s_recv.at[0])
    own_back = pltpu.make_async_copy(message(back, 0), message(ret, 0), r_recv.at[0])

    def partner_copy(n):
        source, target = weights[n]
        return pltpu.make_async_remote_copy(
            src_ref=source,
            dst_ref=target.at[tp],
            send_sem=w_send.at[n],
            recv_sem=w_recv.at[n],
            device_id=(ep, 1 - tp),
            device_id_type=MESH,
        )

    def chunk_slice(i):
        return pl.ds(pl.multiple_of(i * chunk_slabs, chunk_slabs), chunk_slabs)

    def dispatch(i, carry):
        which = place[pl.ds(pl.multiple_of(i * chunk_rows, chunk_rows), chunk_rows), :]
        for n in range(width // 512):
            columns = slice(n * 512, (n + 1) * 512)
            sent = jnp.dot(which, normed[:, columns], preferred_element_type=jnp.float32)
            send[chunk_slice(i), :, columns] = sent.astype(jnp.bfloat16).reshape(
                chunk_slabs, SLAB, 512
            )

        @pl.when(i == 0)
        def _():
            own_out.start()

        def go(o, carry):
            outgoing(o).start()
            return carry

        lax.fori_loop(jnp.maximum(i * per, 1), (i + 1) * per, go, 0)

        @pl.when(i == 0)
        def _():
            for n in range(3):
                partner_copy(n).start()

        return carry

    lax.fori_loop(0, chunks, dispatch, 0)

    up0, up1 = upright(target0), upright(target1)
    slot_columns = lax.broadcasted_iota(jnp.int32, (tokens, chunk_rows), 1).astype(jnp.float32)
    for i in range(chunks):
        pick0[i] = jnp.where(slot_columns + float(i * chunk_rows) == up0, 1.0, 0.0).astype(
            jnp.bfloat16
        )
        pick1[i] = jnp.where(slot_columns + float(i * chunk_rows) == up1, 1.0, 0.0).astype(
            jnp.bfloat16
        )
    weight0, weight1 = upright(route[0:1, :]), upright(route[1:2, :])

    for n in range(2):
        pltpu.make_async_copy(weights[n][0], weights[n][1].at[tp], w_load.at[n]).wait()
        partner_copy(n).wait_recv()

    def serve(i, carry):
        def arrive(o, carry):
            outgoing(o).wait_recv()
            return carry

        @pl.when(i == 0)
        def _():
            own_out.wait()

        lax.fori_loop(jnp.maximum(i * per, 1), (i + 1) * per, arrive, 0)
        rows[...] = recv[chunk_slice(i)].reshape(chunk_rows, width)

        for h in range(2):

            def expand(n, carry):
                columns = pl.ds(pl.multiple_of(n * TILE, TILE), TILE)
                gate = jnp.dot(rows[...], wg[h, :, columns], preferred_element_type=jnp.float32)
                up = jnp.dot(rows[...], wu[h, :, columns], preferred_element_type=jnp.float32)
                gate = jnp.minimum(gate, LIMIT)
                up = jnp.clip(up, -LIMIT, LIMIT)
                hidden[h, :, columns] = (
                    (up + 1.0) * gate * jax.nn.sigmoid(ALPHA * gate)
                ).astype(jnp.bfloat16)
                return carry

            lax.fori_loop(0, half // TILE, expand, 0)

        @pl.when(i == 0)
        def _():
            pltpu.make_async_copy(weights[2][0], weights[2][1].at[tp], w_load.at[2]).wait()
            partner_copy(2).wait_recv()

        def contract(n, carry):
            columns = pl.ds(pl.multiple_of(n * TILE, TILE), TILE)
            part0 = jnp.dot(hidden[0], wd[0, :, columns], preferred_element_type=jnp.float32)
            part1 = jnp.dot(hidden[1], wd[1, :, columns], preferred_element_type=jnp.float32)
            both = part0.astype(jnp.bfloat16).astype(jnp.float32) + part1.astype(
                jnp.bfloat16
            ).astype(jnp.float32)
            back[chunk_slice(i), :, columns] = both.astype(jnp.bfloat16).reshape(
                chunk_slabs, SLAB, TILE
            )
            return carry

        lax.fori_loop(0, width // TILE, contract, 0)

        @pl.when(i == 0)
        def _():
            own_back.start()

        def go(o, carry):
            returning(o).start()
            return carry

        lax.fori_loop(jnp.maximum(i * per, 1), (i + 1) * per, go, 0)
        return carry

    lax.fori_loop(0, chunks, serve, 0)

    def collect(i, carry):
        def arrive(o, carry):
            returning(o).wait_recv()
            return carry

        @pl.when(i == 0)
        def _():
            own_back.wait()

        lax.fori_loop(jnp.maximum(i * per, 1), (i + 1) * per, arrive, 0)
        for n in range(width // 512):
            columns = slice(n * 512, (n + 1) * 512)
            came = ret[chunk_slice(i), :, columns].reshape(chunk_rows, 512)
            mine = (
                jnp.dot(pick0[i], came, preferred_element_type=jnp.float32) * weight0
                + jnp.dot(pick1[i], came, preferred_element_type=jnp.float32) * weight1
            )

            @pl.when(i == 0)
            def _():
                total[:, columns] = mine

            @pl.when(i > 0)
            def _():
                total[:, columns] += mine

        return carry

    lax.fori_loop(0, chunks, collect, 0)

    post_gain = post_ref[...]

    def finish(i, carry):
        here = pl.ds(pl.multiple_of(i * step_rows, step_rows), step_rows)
        out_ref[here, :] = norm_rows(total[here, :], post_gain).astype(jnp.bfloat16)
        return carry

    lax.fori_loop(0, tokens // step_rows, finish, 0)

    def sent(o, carry):
        outgoing(o).wait_send()
        returning(o).wait_send()
        return carry

    lax.fori_loop(1, N_EP, sent, 0)
    for n in range(3):
        partner_copy(n).wait_send()


def local(inputs, pre_gain, expert_ids, route_weights, gate_proj, up_proj, down_proj, post_gain):
    tokens, width = inputs.shape
    half = gate_proj.shape[2]
    chunks = 4
    chunk_rows = N_EP // chunks * CAP
    slabs = N_EP * SLABS
    bf16, f32 = jnp.bfloat16, jnp.float32
    vmem = pl.BlockSpec(memory_space=pltpu.VMEM)
    hbm = pl.BlockSpec(memory_space=pl.ANY)
    dma = pltpu.SemaphoreType.DMA
    return pl.pallas_call(
        functools.partial(kernel, chunks),
        out_shape=jax.ShapeDtypeStruct((tokens, width), bf16),
        in_specs=[hbm, vmem, vmem, vmem, hbm, hbm, hbm, vmem],
        out_specs=vmem,
        scratch_shapes=[
            pltpu.VMEM((tokens, width), bf16),
            pltpu.VMEM((tokens, width), bf16),
            pltpu.VMEM((N_EP * CAP, tokens), bf16),
            pltpu.VMEM((chunks, tokens, chunk_rows), bf16),
            pltpu.VMEM((chunks, tokens, chunk_rows), bf16),
            pltpu.VMEM((slabs, SLAB, width), bf16),
            pltpu.VMEM((slabs, SLAB, width), bf16),
            pltpu.VMEM((2, width, half), bf16),
            pltpu.VMEM((2, width, half), bf16),
            pltpu.VMEM((2, half, width), bf16),
            pltpu.VMEM((chunk_rows, width), bf16),
            pltpu.VMEM((2, chunk_rows, half), bf16),
            pltpu.VMEM((slabs, SLAB, width), bf16),
            pltpu.VMEM((slabs, SLAB, width), bf16),
            pltpu.VMEM((tokens, width), f32),
            dma,
            dma((3,)),
            dma((3,)),
            dma((3,)),
            dma((N_EP,)),
            dma((N_EP,)),
            dma((N_EP,)),
            dma((N_EP,)),
        ],
        compiler_params=pltpu.CompilerParams(
            collective_id=0, has_side_effects=True, vmem_limit_bytes=60 * 1024 * 1024
        ),
    )(
        inputs,
        pre_gain.reshape(1, width),
        expert_ids.T,
        route_weights.T,
        gate_proj[0],
        up_proj[0],
        down_proj[0],
        post_gain.reshape(1, width),
    )


def solution(mesh):
    in_specs = (
        P(("ep", "tp"), None),
        P(),
        P(("ep", "tp"), None),
        P(("ep", "tp"), None),
        P("ep", None, "tp"),
        P("ep", None, "tp"),
        P("ep", "tp", None),
        P(),
    )
    out_specs = P(("ep", "tp"), None)
    return jax.shard_map(local, mesh=mesh, in_specs=in_specs, out_specs=out_specs, check_vma=False)
```

profile of v0, /device:TPU:10, one launch (start us, length us, event | category | flops | bytes accessed | tf_op | source)
XLA Modules:
  0.0 101.9 jit_solution(2289008340400087405)
XLA Ops:
  0.0 99.6 %shard_map.82 = bf16[256,2048]{1,0:T(8,128)(2,1)} custom-call(bf16[256,2048]{1,0:T(8,128)(2,1)} %x_ref.1, f32[1,2048]{1,0:T(1,128)} %bitcast.10, s32[2,256]{1,0:T(2,128)} %bitcast.12, f32[2,256]{1,0:T(2,128)} %bitcast.13, bf16[2048,1024]{1,0:T(8,128)(2,1)} %bitcast.7, bf16[2048,1024]{1,0:T(8,128)(2,1)} %bitcast.8, bf16[1024,2048]{1,0:T(8,128)(2,1)} %bitcast.9, ...), custom_call_target="tpu_custom_call" | custom-call | tf_op jit(solution)/shard_map/pallas_call | solution.py:343
  99.6 2.3 %copy.10 = bf16[256,2048]{1,0:T(8,128)(2,1)} copy(bf16[256,2048]{1,0:T(8,128)(2,1)} %shard_map.82) | data formatting | bytes 2097152
where the time goes:
time: 102 us
  Pallas kernels  99.6 us (98%)
  local copies, waits for them, and re-layouts  2.3 us (2%)
    pallas_call x1, Pallas kernels, local(): pl.pallas_call(functools.partial(kernel, chunks), out_shape=jax.ShapeDtyp...  99.6 us
    unnamed x1, local copies, waits for them, and re-layouts  2.3 us

commit v1 on v0

--- a/solution.py
+++ b/solution.py
@@ -25,7 +25,7 @@
 
 def offset_device(ep, o, sign):
     a, b, c = o % 4, (o // 4) % 4, o // 16
-    ox, oy, oz = a, (b + a) % 4, (c + b) % 4
+    ox, oy, oz = a, (a + b) % 4, (a + b + c) % 4
     x, y, z = ep % 4, (ep // 4) % 4, ep // 16
     return (
         ((z + sign * oz + 4) % 4) * 16 + ((y + sign * oy + 4) % 4) * 4 + (x + sign * ox + 4) % 4
@@ -110,7 +110,7 @@
     x_me, y_me, z_me = ep % 4, (ep // 4) % 4, ep // 16
     a = (ids % 4 - x_me + 4) % 4
     b = ((ids // 4) % 4 - y_me - a + 8) % 4
-    c = (ids // 16 - z_me - b + 8) % 4
+    c = (ids // 16 - z_me - a - b + 12) % 4
     order = (a + 4 * b + 16 * c).astype(jnp.float32) * float(CAP)
     target0 = order[0:1, :] + slot0
     target1 = order[1:2, :] + slot1
@@ -137,7 +137,6 @@
 
     lax.fori_loop(0, tokens // step_rows, norm_step, 0)
 
-    pl.semaphore_wait(barrier, N_EP)
 
     def message(buffer, o):
         return buffer.at[pl.ds(o * SLABS, SLABS)]
@@ -190,6 +189,7 @@
 
         @pl.when(i == 0)
         def _():
+            pl.semaphore_wait(barrier, N_EP)
             own_out.start()
 
         def go(o, carry):
@@ -255,18 +255,18 @@
             partner_copy(2).wait_recv()
 
         def contract(n, carry):
-            columns = pl.ds(pl.multiple_of(n * TILE, TILE), TILE)
+            columns = pl.ds(pl.multiple_of(n * 512, 512), 512)
             part0 = jnp.dot(hidden[0], wd[0, :, columns], preferred_element_type=jnp.float32)
             part1 = jnp.dot(hidden[1], wd[1, :, columns], preferred_element_type=jnp.float32)
             both = part0.astype(jnp.bfloat16).astype(jnp.float32) + part1.astype(
                 jnp.bfloat16
             ).astype(jnp.float32)
             back[chunk_slice(i), :, columns] = both.astype(jnp.bfloat16).reshape(
-                chunk_slabs, SLAB, TILE
+                chunk_slabs, SLAB, 512
             )
             return carry
 
-        lax.fori_loop(0, width // TILE, contract, 0)
+        lax.fori_loop(0, width // 512, contract, 0)
 
         @pl.when(i == 0)
         def _():
@@ -342,7 +342,7 @@
     dma = pltpu.SemaphoreType.DMA
     return pl.pallas_call(
         functools.partial(kernel, chunks),
-        out_shape=jax.ShapeDtypeStruct((tokens, width), bf16),
+        out_shape=pltpu.VMEM((tokens, width), bf16),
         in_specs=[hbm, vmem, vmem, vmem, hbm, hbm, hbm, vmem],
         out_specs=vmem,
         scratch_shapes=[

time: 102 us -> 88.1 us (0.86); the launches traced: 102 us -> 86.4 us
  Pallas kernels: 99.6 us -> 85.4 us
  local copies, waits for them, and re-layouts: 2.3 us -> 0.97 us
    pallas_call x1, Pallas kernels: 99.6 us -> 85.4 us  [local(): pl.pallas_call(functools.partial(kernel, chunks), out_shape=pltpu.VMEM((t...]
    unnamed x1, local copies, waits for them, and re-layouts: 2.3 us -> 0.97 us
where the time goes in v1:
time: 88.1 us; the launch traced here: 86.4 us
  Pallas kernels  85.4 us (97%)
  local copies, waits for them, and re-layouts  0.97 us (1%)
    pallas_call x1, Pallas kernels, local(): pl.pallas_call(functools.partial(kernel, chunks), out_shape=pltpu.VMEM((t...  85.4 us

profile of v1, /device:TPU:10, one launch (start us, length us, event | category | flops | bytes accessed | tf_op | source)
XLA Modules:
  0.0 86.4 jit_solution(9349462668469696770)
XLA Ops:
  0.0 85.4 %shard_map.82 = bf16[256,2048]{1,0:T(8,128)(2,1)S(1)} custom-call(bf16[256,2048]{1,0:T(8,128)(2,1)} %x_ref.1, f32[1,2048]{1,0:T(1,128)} %bitcast.10, s32[2,256]{1,0:T(2,128)} %bitcast.12, f32[2,256]{1,0:T(2,128)} %bitcast.13, bf16[2048,1024]{1,0:T(8,128)(2,1)} %bitcast.7, bf16[2048,1024]{1,0:T(8,128)(2,1)} %bitcast.8, bf16[1024,2048]{1,0:T(8,128)(2,1)} %bitcast.9, ...), custom_call_target="tpu_custom_call" | custom-call | tf_op jit(solution)/shard_map/pallas_call | solution.py:343
  85.4 1.0 %copy.10 = bf16[256,2048]{1,0:T(8,128)(2,1)} copy(bf16[256,2048]{1,0:T(8,128)(2,1)S(1)} %shard_map.82) | data formatting | bytes 2097152

commit v2 on v1

--- a/solution.py
+++ b/solution.py
@@ -17,6 +17,7 @@
 SLAB = 4
 SLABS = CAP // SLAB
 TILE = 256
+PARTS = 2
 
 
 def norm_rows(floats, gain):
@@ -161,6 +162,17 @@
             device_id_type=MESH,
         )
 
+    def returning_part(o, n):
+        columns = pl.ds(n * (width // PARTS), width // PARTS)
+        return pltpu.make_async_remote_copy(
+            src_ref=back.at[pl.ds(o * SLABS, SLABS), :, columns],
+            dst_ref=ret.at[pl.ds(o * SLABS, SLABS), :, columns],
+            send_sem=r_send.at[o + n * per],
+            recv_sem=r_recv.at[o + n * per],
+            device_id=(offset_device(ep, o, -1), tp),
+            device_id_type=MESH,
+        )
+
     own_out = pltpu.make_async_copy(message(send, 0), message(recv, 0), s_recv.at[0])
     own_back = pltpu.make_async_copy(message(back, 0), message(ret, 0), r_recv.at[0])
 
@@ -276,13 +288,42 @@
             returning(o).start()
             return carry
 
-        lax.fori_loop(jnp.maximum(i * per, 1), (i + 1) * per, go, 0)
+        @pl.when(i < chunks - 1)
+        def _():
+            lax.fori_loop(jnp.maximum(i * per, 1), (i + 1) * per, go, 0)
+
+        @pl.when(i == chunks - 1)
+        def _():
+            for n in range(PARTS):
+
+                def go_part(o, carry):
+                    returning_part(o, n).start()
+                    return carry
+
+                lax.fori_loop(N_EP - per, N_EP, go_part, 0)
+
         return carry
 
     lax.fori_loop(0, chunks, serve, 0)
+
+    def sent(o, carry):
+        outgoing(o).wait_send()
+        return carry
+
+    lax.fori_loop(1, N_EP, sent, 0)
+    for n in range(3):
+        partner_copy(n).wait_send()
+
+    def mixed(i, n):
+        came = ret[chunk_slice(i), :, n * 512 : (n + 1) * 512].reshape(chunk_rows, 512)
+        return (
+            jnp.dot(pick0[i], came, preferred_element_type=jnp.float32) * weight0
+            + jnp.dot(pick1[i], came, preferred_element_type=jnp.float32) * weight1
+        )
 
     def collect(i, carry):
         def arrive(o, carry):
+            returning(o).wait_send()
             returning(o).wait_recv()
             return carry
 
@@ -292,12 +333,8 @@
 
         lax.fori_loop(jnp.maximum(i * per, 1), (i + 1) * per, arrive, 0)
         for n in range(width // 512):
+            mine = mixed(i, n)
             columns = slice(n * 512, (n + 1) * 512)
-            came = ret[chunk_slice(i), :, columns].reshape(chunk_rows, 512)
-            mine = (
-                jnp.dot(pick0[i], came, preferred_element_type=jnp.float32) * weight0
-                + jnp.dot(pick1[i], came, preferred_element_type=jnp.float32) * weight1
-            )
 
             @pl.when(i == 0)
             def _():
@@ -309,25 +346,28 @@
 
         return carry
 
-    lax.fori_loop(0, chunks, collect, 0)
+    lax.fori_loop(0, chunks - 1, collect, 0)
 
     post_gain = post_ref[...]
-
-    def finish(i, carry):
-        here = pl.ds(pl.multiple_of(i * step_rows, step_rows), step_rows)
-        out_ref[here, :] = norm_rows(total[here, :], post_gain).astype(jnp.bfloat16)
-        return carry
-
-    lax.fori_loop(0, tokens // step_rows, finish, 0)
-
-    def sent(o, carry):
-        outgoing(o).wait_send()
-        returning(o).wait_send()
-        return carry
-
-    lax.fori_loop(1, N_EP, sent, 0)
-    for n in range(3):
-        partner_copy(n).wait_send()
+    squares = jnp.zeros((tokens, 1), jnp.float32)
+    last = chunks - 1
+    for h in range(PARTS):
+
+        def arrive_part(o, carry):
+            returning_part(o, h).wait_send()
+            returning_part(o, h).wait_recv()
+            return carry
+
+        lax.fori_loop(last * per, N_EP, arrive_part, 0)
+        for n in range(h * width // 512 // PARTS, (h + 1) * width // 512 // PARTS):
+            columns = slice(n * 512, (n + 1) * 512)
+            part = total[:, columns] + mixed(last, n)
+            total[:, columns] = part
+            squares += jnp.sum(part * part, axis=1, keepdims=True)
+    scale = lax.rsqrt(squares / float(width) + EPSILON)
+    for n in range(width // 512):
+        columns = slice(n * 512, (n + 1) * 512)
+        out_ref[:, columns] = (total[:, columns] * scale * post_gain[:, columns]).astype(jnp.bfloat16)
 
 
 def local(inputs, pre_gain, expert_ids, route_weights, gate_proj, up_proj, down_proj, post_gain):
@@ -367,8 +407,8 @@
             dma((3,)),
             dma((N_EP,)),
             dma((N_EP,)),
-            dma((N_EP,)),
-            dma((N_EP,)),
+            dma((N_EP + (PARTS - 1) * N_EP // chunks,)),
+            dma((N_EP + (PARTS - 1) * N_EP // chunks,)),
         ],
         compiler_params=pltpu.CompilerParams(
             collective_id=0, has_side_effects=True, vmem_limit_bytes=60 * 1024 * 1024

time: 88.1 us -> 86 us (0.976)
  Pallas kernels: 85.4 us -> 83.5 us
    pallas_call x1, Pallas kernels: 85.4 us -> 83.5 us  [local(): pl.pallas_call(functools.partial(kernel, chunks), out_shape=pltpu.VMEM((t...]
where the time goes in v2:
time: 86 us; the launch traced here: 84.5 us
  Pallas kernels  83.5 us (97%)
  local copies, waits for them, and re-layouts  0.97 us (1%)
    pallas_call x1, Pallas kernels, local(): pl.pallas_call(functools.partial(kernel, chunks), out_shape=pltpu.VMEM((t...  83.5 us

profile of v2, /device:TPU:10, one launch (start us, length us, event | category | flops | bytes accessed | tf_op | source)
XLA Modules:
  0.0 84.5 jit_solution(6015516797440742243)
XLA Ops:
  0.0 83.5 %shard_map.82 = bf16[256,2048]{1,0:T(8,128)(2,1)S(1)} custom-call(bf16[256,2048]{1,0:T(8,128)(2,1)} %x_ref.1, f32[1,2048]{1,0:T(1,128)} %bitcast.10, s32[2,256]{1,0:T(2,128)} %bitcast.12, f32[2,256]{1,0:T(2,128)} %bitcast.13, bf16[2048,1024]{1,0:T(8,128)(2,1)} %bitcast.7, bf16[2048,1024]{1,0:T(8,128)(2,1)} %bitcast.8, bf16[1024,2048]{1,0:T(8,128)(2,1)} %bitcast.9, ...), custom_call_target="tpu_custom_call" | custom-call | tf_op jit(solution)/shard_map/pallas_call | solution.py:383
  83.5 1.0 %copy.10 = bf16[256,2048]{1,0:T(8,128)(2,1)} copy(bf16[256,2048]{1,0:T(8,128)(2,1)S(1)} %shard_map.82) | data formatting | bytes 2097152

commit v3 on v2

--- a/solution.py
+++ b/solution.py
@@ -47,8 +47,7 @@
     x_buf,
     normed,
     place,
-    pick0,
-    pick1,
+    picks,
     send,
     recv,
     wg,
@@ -222,10 +221,10 @@
     up0, up1 = upright(target0), upright(target1)
     slot_columns = lax.broadcasted_iota(jnp.int32, (tokens, chunk_rows), 1).astype(jnp.float32)
     for i in range(chunks):
-        pick0[i] = jnp.where(slot_columns + float(i * chunk_rows) == up0, 1.0, 0.0).astype(
+        picks[i, :tokens, :] = jnp.where(slot_columns + float(i * chunk_rows) == up0, 1.0, 0.0).astype(
             jnp.bfloat16
         )
-        pick1[i] = jnp.where(slot_columns + float(i * chunk_rows) == up1, 1.0, 0.0).astype(
+        picks[i, tokens:, :] = jnp.where(slot_columns + float(i * chunk_rows) == up1, 1.0, 0.0).astype(
             jnp.bfloat16
         )
     weight0, weight1 = upright(route[0:1, :]), upright(route[1:2, :])
@@ -316,9 +315,9 @@
 
     def mixed(i, n):
         came = ret[chunk_slice(i), :, n * 512 : (n + 1) * 512].reshape(chunk_rows, 512)
+        both = jnp.dot(picks[i], came, preferred_element_type=jnp.float32)
         return (
-            jnp.dot(pick0[i], came, preferred_element_type=jnp.float32) * weight0
-            + jnp.dot(pick1[i], came, preferred_element_type=jnp.float32) * weight1
+            both[:tokens] * weight0 + both[tokens:] * weight1
         )
 
     def collect(i, carry):
@@ -389,8 +388,7 @@
             pltpu.VMEM((tokens, width), bf16),
             pltpu.VMEM((tokens, width), bf16),
             pltpu.VMEM((N_EP * CAP, tokens), bf16),
-            pltpu.VMEM((chunks, tokens, chunk_rows), bf16),
-            pltpu.VMEM((chunks, tokens, chunk_rows), bf16),
+            pltpu.VMEM((chunks, 2 * tokens, chunk_rows), bf16),
             pltpu.VMEM((slabs, SLAB, width), bf16),
             pltpu.VMEM((slabs, SLAB, width), bf16),
             pltpu.VMEM((2, width, half), bf16),

time: 86 us -> 86 us (level)
  no operation moved by 1% of the time
where the time goes in v3:
time: 86 us; the launch traced here: 84.5 us
  Pallas kernels  83.5 us (97%)
  local copies, waits for them, and re-layouts  0.97 us (1%)
    pallas_call x1, Pallas kernels, local(): pl.pallas_call(functools.partial(kernel, chunks), out_shape=pltpu.VMEM((t...  83.5 us

profile of v3, /device:TPU:10, one launch (start us, length us, event | category | flops | bytes accessed | tf_op | source)
XLA Modules:
  0.0 84.5 jit_solution(9150269168933020897)
XLA Ops:
  0.0 83.5 %shard_map.82 = bf16[256,2048]{1,0:T(8,128)(2,1)S(1)} custom-call(bf16[256,2048]{1,0:T(8,128)(2,1)} %x_ref.1, f32[1,2048]{1,0:T(1,128)} %bitcast.10, s32[2,256]{1,0:T(2,128)} %bitcast.12, f32[2,256]{1,0:T(2,128)} %bitcast.13, bf16[2048,1024]{1,0:T(8,128)(2,1)} %bitcast.7, bf16[2048,1024]{1,0:T(8,128)(2,1)} %bitcast.8, bf16[1024,2048]{1,0:T(8,128)(2,1)} %bitcast.9, ...), custom_call_target="tpu_custom_call" | custom-call | tf_op jit(solution)/shard_map/pallas_call | solution.py:382
  83.5 1.0 %copy.10 = bf16[256,2048]{1,0:T(8,128)(2,1)} copy(bf16[256,2048]{1,0:T(8,128)(2,1)S(1)} %shard_map.82) | data formatting | bytes 2097152
